TPU v7x, 32 devices: a whole 2x2x4 slice. The times are simulated.
32 devices in a mesh: sp: 8 (over z, y), dp: 4 (over x, core).
Axes of the slice: x: 2, y: 2, z: 4, core: 2. Of those that a mesh axis runs over, the one named last changes fastest.
Arguments:
- resid: bfloat16 [4, 2048, 2048], P('dp', 'sp'), may hold values from -6 to 6
- mixer_inputs: bfloat16 [4, 2048, 4096], P('dp', 'sp'), may hold values from -6 to 6
- output_gate: bfloat16 [4, 2048, 4096], P('dp', 'sp'), may hold values from -6 to 6
- write_rows_input: bfloat16 [4, 2048, 256], P('dp', 'sp'), may hold values from -6 to 6
- read_rows_input: bfloat16 [4, 2048, 256], P('dp', 'sp'), may hold values from -6 to 6
- step_size_logits: bfloat16 [4, 2048, 64, 2], P('dp', 'sp'), may hold values from -5 to 5
- extra_log_decay: bfloat16 [4, 2048, 64, 2], P('dp', 'sp'), may hold values from -0.7 to 0
- mixer_conv_taps: bfloat16 [5, 4096], P(None, 'sp'), may hold values from -2.5 to 2.5
- write_conv_taps: bfloat16 [5, 256], replicated, may hold values from -2.5 to 2.5
- read_conv_taps: bfloat16 [5, 256], replicated, may hold values from -2.5 to 2.5
- step_size_bias: float32 [64, 2], P('sp'), may hold values from -20 to -3
- decay_speed: float32 [64, 2], P('sp'), may hold values from 1 to 16
- grouped_norm_gain: float32 [4096], replicated, may hold values from 0.1 to 1.9
- output_matrix: bfloat16 [4096, 2048], P(None, 'dp'), may hold values from -0.09375 to 0.09375
- output_gain: float32 [2048], replicated, may hold values from 0.1 to 1.9
- feedforward_gain: float32 [2048], replicated, may hold values from 0.1 to 1.9
- routes: int32 [4, 2048, 2], P('dp', 'sp'), may hold values from 0 to 7, all different within a row; in each aligned block of 256 rows (0 to 255, 256 to 511, ..., all dimensions but the last counted through in order) at most 96 rows name the same one
- route_weights: float32 [4, 2048, 2], P('dp', 'sp'), may hold values from 0.1 to 1
- expert_gate_weight: bfloat16 [8, 2048, 1024], P('sp'), may hold values from -0.125 to 0.125
- expert_up_weight: bfloat16 [8, 2048, 1024], P('sp'), may hold values from -0.125 to 0.125
- expert_down_weight: bfloat16 [8, 1024, 2048], P('sp'), may hold values from -0.1875 to 0.1875
- expert_sum_gain: float32 [2048], replicated, may hold values from 0.1 to 1.9
Outputs:
- mixed_out: bfloat16 [4, 2048, 2048], P('dp', 'sp')
Inputs may be any that keep to these rules, and one draw needn't show every extreme that they name: `routes`: each token names 2 different experts; the 256 positions of one device name one expert at most 96 times, a bound that some block reaches.
All inputs are finite; a program needn't handle non-finite values.
Results may differ from a plain program's by a relative error of at most 0.012.
Values may be sent and summed in bfloat16 or wider, within the bound.
A program may use at most 128 MiB of HBM per device.

v0:
```python
import jax
import jax.numpy as jnp
from jax import lax
from jax.sharding import PartitionSpec as P

D = 2048
HEADS = 64
HEAD_DIM = 64
GROUPS = 2
STATE = 128
BLOCK = 128
TOPK = 2
INNER = 4096


EPS = 1e-06


def rms_scale(values, scale_gain):
    return values * lax.rsqrt(jnp.mean(values * values, axis=-1, keepdims=True) + EPS) * scale_gain


def centred_conv(values, kernel):
    span_len = kernel.shape[0]
    half_span = span_len // 2
    length = values.shape[0]
    padded = jnp.pad(values.astype(jnp.float32), ((half_span, half_span), (0, 0)))
    summed = jnp.zeros(values.shape, jnp.float32)
    for offset in range(span_len):
        summed = summed + padded[offset : offset + length] * kernel[offset].astype(jnp.float32)
    return jax.nn.silu(summed).astype(jnp.bfloat16)


def block_pass(inputs, writes, read_rows, head_step_sizes, logarithm_decay):
    length = inputs.shape[0]
    blocks = length // BLOCK
    inp_block = inputs.reshape(blocks, BLOCK, -1)
    wr_block = writes.reshape(blocks, BLOCK, -1)
    rd_block = read_rows.reshape(blocks, BLOCK, -1)
    step_blk = head_step_sizes.reshape(blocks, BLOCK)
    cumulative = jnp.cumsum(logarithm_decay.reshape(blocks, BLOCK), axis=1)
    lower_tri = jnp.tril(jnp.ones((BLOCK, BLOCK), dtype=bool))
    spread = cumulative[:, :, None] - cumulative[:, None, :]
    in_block = jnp.where(lower_tri, jnp.exp(jnp.where(lower_tri, spread, 0.0)), 0.0)
    scores = jnp.einsum("cln,csn->cls", rd_block, wr_block, preferred_element_type=jnp.float32)
    weights = (scores * in_block * step_blk[:, None, :]).astype(jnp.bfloat16)
    within = jnp.einsum("cls,csp->clp", weights, inp_block, preferred_element_type=jnp.float32)
    to_end = jnp.exp(cumulative[:, -1:] - cumulative) * step_blk
    scaled = (wr_block.astype(jnp.float32) * to_end[:, :, None]).astype(jnp.bfloat16)
    states = jnp.einsum("csn,csp->cnp", scaled, inp_block, preferred_element_type=jnp.float32)
    totals = cumulative[:, -1]
    through = jnp.cumsum(totals)
    preceding = through - totals
    strict = jnp.tril(jnp.ones((blocks, blocks), dtype=bool), -1)
    carry_mat = jnp.where(
        strict, jnp.exp(jnp.where(strict, preceding[:, None] - through[None, :], 0.0)), 0.0
    )
    entering = jnp.dot(carry_mat, states.reshape(blocks, -1), precision=lax.Precision.HIGHEST)
    entering = entering.reshape(states.shape).astype(jnp.bfloat16)
    carried = (
        jnp.einsum("cln,cnp->clp", rd_block, entering, preferred_element_type=jnp.float32)
        * jnp.exp(cumulative)[:, :, None]
    )
    return (within + carried).reshape(length, -1)


def both_ways(inputs, writes, read_rows, head_step_sizes, logarithm_decay):
    forward = block_pass(inputs, writes, read_rows, head_step_sizes[:, 0], logarithm_decay[:, 0])
    backward = block_pass(
        jnp.flip(inputs, 0),
        jnp.flip(writes, 0),
        jnp.flip(read_rows, 0),
        jnp.flip(head_step_sizes[:, 1], 0),
        jnp.flip(logarithm_decay[:, 1], 0),
    )
    return forward + jnp.flip(backward, 0)


def head_result(packed_head):
    return both_ways(*packed_head).astype(jnp.bfloat16)


def local(
    resid,
    mixer_inputs,
    output_gate,
    write_rows_input,
    read_rows_input,
    step_size_logits,
    extra_log_decay,
    mixer_conv_taps,
    write_conv_taps,
    read_conv_taps,
    step_size_bias,
    decay_speed,
    grouped_norm_gain,
    output_matrix,
    output_gain,
    feedforward_gain,
    routes,
    route_weights,
    expert_gate_weight,
    expert_up_weight,
    expert_down_weight,
    expert_sum_gain,
):
    tok_rows = mixer_inputs.shape[1]
    local_heads = step_size_bias.shape[0]
    per_group = HEADS // GROUPS
    first_head = lax.axis_index("sp") * local_heads
    group_id = first_head // per_group
    heads_x = mixer_inputs[0].reshape(tok_rows, HEADS, HEAD_DIM)
    shifted_inputs, shifted_step_pre, shifted_extra_decay = (
        lax.all_to_all(heads_x, "sp", split_axis=1, concat_axis=0, tiled=True),
        lax.all_to_all(step_size_logits[0], "sp", split_axis=1, concat_axis=0, tiled=True),
        lax.all_to_all(extra_log_decay[0], "sp", split_axis=1, concat_axis=0, tiled=True),
    )
    seq_len = shifted_inputs.shape[0]
    whole_write, whole_read = (
        lax.all_gather(write_rows_input[0], "sp", axis=0, tiled=True),
        lax.all_gather(read_rows_input[0], "sp", axis=0, tiled=True),
    )
    col_start = group_id * STATE
    write_act = centred_conv(
        lax.dynamic_slice_in_dim(whole_write, col_start, STATE, 1),
        lax.dynamic_slice_in_dim(write_conv_taps, col_start, STATE, 1),
    )
    read_act = centred_conv(
        lax.dynamic_slice_in_dim(whole_read, col_start, STATE, 1),
        lax.dynamic_slice_in_dim(read_conv_taps, col_start, STATE, 1),
    )
    write_heads = jnp.broadcast_to(write_act[:, None, :], (seq_len, local_heads, STATE))
    read_heads = jnp.broadcast_to(read_act[:, None, :], (seq_len, local_heads, STATE))
    x_act = centred_conv(shifted_inputs.reshape(seq_len, local_heads * HEAD_DIM), mixer_conv_taps)
    x_act = x_act.reshape(seq_len, local_heads, HEAD_DIM)
    head_step_sizes = jax.nn.softplus(shifted_step_pre.astype(jnp.float32) + step_size_bias)
    logarithm_decay = shifted_extra_decay.astype(jnp.float32) - decay_speed * head_step_sizes
    by_head = tuple(
        (
            jnp.moveaxis(item, 1, 0)
            for item in (x_act, write_heads, read_heads, head_step_sizes, logarithm_decay)
        )
    )
    head_outputs = jnp.moveaxis(lax.map(head_result, by_head), 0, 1)
    token_heads = lax.all_to_all(head_outputs, "sp", split_axis=0, concat_axis=1, tiled=True)
    gated_vals = token_heads.reshape(tok_rows, INNER).astype(jnp.float32) * jax.nn.silu(
        output_gate[0].astype(jnp.float32)
    )
    grouped = gated_vals.reshape(tok_rows, GROUPS, -1)
    grouped = grouped * lax.rsqrt(jnp.mean(grouped * grouped, axis=-1, keepdims=True) + EPS)
    normed = (grouped.reshape(tok_rows, -1) * grouped_norm_gain).astype(jnp.bfloat16)
    projected = jnp.dot(
        normed,
        lax.all_gather(output_matrix, "dp", axis=1, tiled=True),
        preferred_element_type=jnp.float32,
    )
    resid_one = (resid[0].astype(jnp.float32) + rms_scale(projected, output_gain)).astype(
        jnp.bfloat16
    )
    ffn_in = rms_scale(resid_one.astype(jnp.float32), feedforward_gain).astype(jnp.bfloat16)
    sp_size = lax.axis_size("sp")
    local_experts = expert_gate_weight.shape[0]
    experts = local_experts * sp_size
    capacity = 3 * tok_rows * TOPK // (2 * experts)
    flat_route = routes[0].reshape(-1)
    one_hot = (flat_route[:, None] == jnp.arange(experts, dtype=jnp.int32)[None, :]).astype(
        jnp.int32
    )
    earlier = jnp.cumsum(one_hot, axis=0) - one_hot
    slot_pos = jnp.sum(earlier * one_hot, axis=1)
    slot_dest = flat_route * capacity + slot_pos
    source_tok = jnp.arange(tok_rows * TOPK, dtype=jnp.int32) // TOPK
    slot_token = jnp.full((experts * capacity,), tok_rows, jnp.int32).at[slot_dest].set(source_tok)
    padded_in = jnp.concatenate([ffn_in, jnp.zeros((1, D), jnp.bfloat16)], axis=0)
    send_rows = padded_in[slot_token].reshape(sp_size, local_experts, capacity, D)
    arrived = lax.all_to_all(send_rows, "sp", split_axis=0, concat_axis=0, tiled=True)
    gate_part = jnp.einsum(
        "sekd,edh->sekh", arrived, expert_gate_weight, preferred_element_type=jnp.float32
    )
    up_part = jnp.einsum(
        "sekd,edh->sekh", arrived, expert_up_weight, preferred_element_type=jnp.float32
    )
    hidden = (jax.nn.silu(gate_part) * up_part).astype(jnp.bfloat16)
    expert_rows = jnp.einsum(
        "sekh,ehd->sekd", hidden, expert_down_weight, preferred_element_type=jnp.float32
    ).astype(jnp.bfloat16)
    returned = lax.all_to_all(expert_rows, "sp", split_axis=0, concat_axis=0, tiled=True)
    picked = returned.reshape(experts * capacity, D)[slot_dest]
    weighted = picked.astype(jnp.float32) * route_weights[0].reshape(-1)[:, None]
    combined = jnp.sum(weighted.reshape(tok_rows, TOPK, D), axis=1)
    mixed_out = resid_one.astype(jnp.float32) + rms_scale(combined, expert_sum_gain)
    return mixed_out.astype(jnp.bfloat16)[None]


def solution(mesh):
    in_specs = (
        P("dp", "sp", None),
        P("dp", "sp", None),
        P("dp", "sp", None),
        P("dp", "sp", None),
        P("dp", "sp", None),
        P("dp", "sp", None, None),
        P("dp", "sp", None, None),
        P(None, "sp"),
        P(),
        P(),
        P("sp", None),
        P("sp", None),
        P(),
        P(None, "dp"),
        P(),
        P(),
        P("dp", "sp", None),
        P("dp", "sp", None),
        P("sp", None, None),
        P("sp", None, None),
        P("sp", None, None),
        P(),
    )
    out_specs = P("dp", "sp", None)
    return jax.shard_map(local, mesh=mesh, in_specs=in_specs, out_specs=out_specs, check_vma=False)
```

profile of v0, /device:TPU:0, one launch (start us, length us, event | category | flops | bytes accessed | tf_op | source)
XLA Modules:
  0.0 578.6 jit_solution(10283695238567507477)
XLA Ops:
  8.0 14.2 %all_to_all.46 = bf16[256,64,2]{0,2,1:T(2,128)(2,1)S(1)} all-to-all(bf16[256,64,2]{0,2,1:T(2,128)(2,1)} %bitcast.401), channel_id=1, replica_groups=mesh['sp'=8,'dp'=4] {'sp'}, dimensions={1} | all-to-all | bytes 131072 | tf_op jit(solution)/shard_map/all_to_all | solution.py:116
  22.2 3.4 all-to-all-start.1
  25.6 4.1 copy.122
  29.7 2.8 all-to-all-done.1
  32.5 3.6 all-to-all-start.2
  38.6 24.9 %all-gather.10.cloned.1.call-done = bf16[1,2048,256]{2,1,0:T(8,128)(2,1)} async-done(((bf16[1,256,256]{2,1,0:T(8,128)(2,1)}), bf16[1,2048,256]{2,1,0:T(8,128)(2,1)}) %all-gather.10.cloned.1.call-update) | async-done | bytes 1048592 | tf_op jit(solution)/shard_map/all_gather | solution.py:120
  63.5 50.5 %all-gather.8.cloned.1.call-done = bf16[1,2048,256]{2,1,0:T(8,128)(2,1)} async-done(((bf16[1,256,256]{2,1,0:T(8,128)(2,1)}), bf16[1,2048,256]{2,1,0:T(8,128)(2,1)}) %all-gather.8.cloned.1.call-update) | async-done | bytes 1048592 | tf_op jit(solution)/shard_map/all_gather | solution.py:121
  118.1 2.0 copy.142
  120.1 7.1 %multiply_convert_fusion.4 = bf16[2048,512]{0,1:T(8,128)(2,1)} fusion(f32[2048,512]{0,1:T(8,128)S(1)} %bitcast.384, f32[512]{0:T(512)S(1)} %bitcast.406, f32[512]{0:T(512)S(1)} %bitcast.407, f32[512]{0:T(512)S(1)} %bitcast.404, f32[512]{0:T(512)S(1)} %bitcast.405, f32[512]{0:T(512)S(1)} %bitcast.403), kind=kLoop, calls=%fused_computation.110 | loop fusion | flops 14680064 | bytes 6301696 | tf_op jit(solution)/shard_map/convert_element_type | solution.py:31
  127.2 3.3 transpose.107
  130.5 2.5 transpose.108
  133.0 142.8 %while.10 = (s32[]{:T(128)}, bf16[8,2048,64]{1,2,0:T(8,128)(2,1)}, bf16[8,2048,128]{2,1,0:T(8,128)(2,1)}, bf16[8,2048,128]{2,1,0:T(8,128)(2,1)}, f32[8,2048,2]{1...) while((s32[]{:T(128)}, bf16[8,2048,64]{1,2,0:T(8,128)(2,1)}, ...), condition=%wide.region_5.6_spmd, body=%wide.region_0.5_spmd.sunk | while | flops 392190464 | bytes 29739348 | solution.py:144
  139.9 1.6 fusion.190
  142.9 1.4 rev.32
  157.8 1.6 fusion.190
  160.8 1.4 rev.32
  175.6 1.6 fusion.190
  178.6 1.4 rev.32
  193.5 1.6 fusion.190
  211.3 1.6 fusion.190
  229.1 1.6 fusion.190
  247.0 1.6 fusion.190
  264.8 1.6 fusion.190
  275.8 5.6 copy.124
  281.4 7.6 %reshape.357 = bf16[8,2,65536]{2,1,0:T(2,128)(2,1)} reshape(bf16[2048,8,64]{2,1,0:T(8,128)(2,1)} %bitcast.383) | data formatting | bytes 4194304
  289.0 4.7 all-to-all-start.3
  294.1 3.3 copy.127
  297.4 2.5 convert.66
  301.6 2.4 scatter_custom_fusion
  304.1 36.6 %all-to-all-done.3 = bf16[8,2,65536]{2,1,0:T(2,128)(2,1)} async-done(((bf16[8,2,65536]{2,1,0:T(2,128)(2,1)}), bf16[8,2,65536]{2,1,0:T(2,128)(2,1)}, u32[]{:S(2)}, u32[]{:S(2)}) %all-to-all-start.3) | async-done | bytes 2097184 | tf_op jit(solution)/shard_map/all_to_all | solution.py:145
  340.7 7.4 %reshape.358 = bf16[2048,8,64]{2,1,0:T(8,128)(2,1)} reshape(bf16[8,2,65536]{2,1,0:T(2,128)(2,1)} %all-to-all-done.3) | data formatting | bytes 4194304
  348.1 5.5 copy.125
  353.6 2.1 convert_element_type.256
  355.7 2.0 copy.143
  357.8 2.0 copy-done
  359.7 3.4 multiply_reduce_fusion.1
  363.2 3.5 copy.126
  366.7 2.8 fusion.72
  369.6 9.2 %multiply_reduce_fusion.3 = (f32[256]{0:T(256)S(1)}, f32[256,2048]{1,0:T(8,128)S(1)}) fusion(bf16[256,4096]{0,1:T(8,128)(2,1)} %fusion.72, bf16[4096,2048]{1,0:T(8,128)(2,1)} %all-gather.6.cloned.1.call-done), kind=kOutput, calls=%fused_computation.134 | convolution fusion | flops 4296015872 | bytes 20972544 | tf_op jit(solution)/shard_map/dot_general | solution.py:152
  380.8 4.3 gather_fusion
  385.1 74.7 %all_to_all.47 = bf16[8,1,96,2048]{3,2,1,0:T(8,128)(2,1)S(1)} all-to-all(bf16[8,1,96,2048]{3,2,1,0:T(8,128)(2,1)} %bitcast.387), channel_id=1, replica_groups=mesh['sp'=8,'dp'=4] {'sp'}, dimensions={0} | all-to-all | bytes 6291456 | tf_op jit(solution)/shard_map/all_to_all | solution.py:176
  459.8 5.1 fusion.67
  464.9 13.0 %fusion.87 = bf16[8,1,96,2048]{3,2,1,0:T(8,128)(2,1)} fusion(bf16[1,1024,2048]{2,1,0:T(8,128)(2,1)} %param.44, f32[8,96,1024]{2,1,0:T(8,128)} %fusion.67, bf16[1,2048,1024]{2,1,0:T(8,128)(2,1)} %param.42, bf16[8,1,96,2048]{3,2,1,0:T(8,128)(2,1)S(1)} %all_to_all.47), kind=kOutput, calls=%fused_computation.126 | convolution fusion | flops 6448742400 | bytes 17825792 | tf_op jit(solution)/shard_map/sekh,ehd->sekd/dot_general | solution.py:184
  478.0 4.1 all-to-all-start.5
  482.2 70.1 %all-to-all-done.5 = bf16[8,1,96,2048]{3,2,1,0:T(8,128)(2,1)S(1)} async-done(((bf16[8,1,96,2048]{3,2,1,0:T(8,128)(2,1)}), bf16[8,1,96,2048]{3,2,1,0:T(8,128)(2,1)S(1)}, u32[]{:S(2)}, u32[]{:S(2)}) %all-to-all-start.5) | async-done | bytes 3145760 | tf_op jit(solution)/shard_map/all_to_all | solution.py:187
  552.3 3.3 gather_fusion.1
  555.6 5.4 reshape.306
  561.1 9.0 %multiply_reduce_fusion = f32[256,2048]{1,0:T(8,128)S(1)} fusion(f32[256,2,2048]{2,1,0:T(2,128)} %reshape.306, f32[256,2]{1,0:T(8,128)S(1)} %copy.135), kind=kLoop, calls=%fused_computation.108 | loop fusion | flops 1572864 | bytes 6293504 | tf_op jit(solution)/shard_map/reduce_sum | solution.py:190
  (411 shorter events, 138.2 us)
Async XLA Ops:
  6.5 56.9 %all-gather.10.cloned.1.call-start = ((), (), s32[]{:S(2)}) async-start(), calls=%async_computation.8 | async-start | bytes 1179648 | tf_op jit(solution)/shard_map/all_gather | solution.py:120
  7.3 106.7 %all-gather.8.cloned.1.call-start = ((), (), s32[]{:S(2)}) async-start(), calls=%async_computation.7 | async-start | bytes 1179648 | tf_op jit(solution)/shard_map/all_gather | solution.py:121
  22.2 10.3 %all-to-all-start.1 = ((bf16[256,64,2]{0,2,1:T(2,128)(2,1)}), bf16[256,64,2]{0,2,1:T(2,128)(2,1)S(1)}, u32[]{:S(2)}, u32[]{:S(2)}) async-start(bf16[256,64,2]{0,2,1:T(2,128)(2,1)} %bitcast.402), calls=%async_computation.1 | async-start | bytes 131072 | tf_op jit(solution)/shard_map/all_to_all | solution.py:115
  32.5 84.4 %all-to-all-start.2 = ((bf16[256,64,64]{0,2,1:T(8,128)(2,1)}), bf16[256,64,64]{0,2,1:T(8,128)(2,1)S(1)}, u32[]{:S(2)}, u32[]{:S(2)}) async-start(bf16[256,64,64]{0,2,1:T(8,128)(2,1)} %bitcast.389), calls=%async_computation.2 | async-start | bytes 4194304 | tf_op jit(solution)/shard_map/all_to_all | solution.py:114
  36.1 0.8 copy-start.15
  36.1 0.9 copy-start.16
  36.1 1.0 copy-start.13
  36.2 1.0 copy-start.14
  36.2 1.0 copy-start.7
  36.2 333.4 %all-gather.6.cloned.1.call-start = ((), (), s32[]{:S(2)}) async-start(), calls=%async_computation.6 | async-start | bytes 20971520 | tf_op jit(solution)/shard_map/all_gather | solution.py:154
  147.9 2.2 copy-start.2
  165.8 2.2 copy-start.2
  183.6 2.2 copy-start.2
  201.5 2.2 copy-start.2
  219.3 2.2 copy-start.2
  237.1 2.2 copy-start.2
  255.0 2.2 copy-start.2
  272.8 2.2 copy-start.2
  289.0 4.7 copy-start.11
  289.0 51.8 %all-to-all-start.3 = ((bf16[8,2,65536]{2,1,0:T(2,128)(2,1)}), bf16[8,2,65536]{2,1,0:T(2,128)(2,1)}, u32[]{:S(2)}, u32[]{:S(2)}) async-start(bf16[8,2,65536]{2,1,0:T(2,128)(2,1)} %reshape.357), calls=%async_computation.3 | async-start | bytes 4194304 | tf_op jit(solution)/shard_map/all_to_all | solution.py:145
  355.7 4.0 copy-start.1
  357.8 2.0 copy-start
  363.2 3.6 copy-start.6
  369.6 9.2 %copy-start.5 = (bf16[1,256,2048]{2,1,0:T(8,128)(2,1)S(1)}, bf16[1,256,2048]{2,1,0:T(8,128)(2,1)}, u32[]{:S(2)}) copy-start(bf16[1,256,2048]{2,1,0:T(8,128)(2,1)} %param.24) | copy-start | bytes 3145732
  369.6 9.2 %copy-start.8 = (f32[2048]{0:T(1024)S(1)}, f32[2048]{0:T(1024)}, u32[]{:S(2)}) copy-start(f32[2048]{0:T(1024)} %param.38) | copy-start | bytes 24580
  378.8 1.6 copy-start.9
  379.4 1.0 copy-start.3
  385.1 74.7 %copy-start.17 = (bf16[1,2048,1024]{2,1,0:T(8,128)(2,1)S(1)}, bf16[1,2048,1024]{2,1,0:T(8,128)(2,1)}, u32[]{:S(2)}) copy-start(bf16[1,2048,1024]{2,1,0:T(8,128)(2,1)} %param.43) | copy-start | bytes 12582916
  477.9 4.1 copy-start.12
  478.0 74.4 %all-to-all-start.5 = ((bf16[8,1,96,2048]{3,2,1,0:T(8,128)(2,1)}), bf16[8,1,96,2048]{3,2,1,0:T(8,128)(2,1)S(1)}, u32[]{:S(2)}, u32[]{:S(2)}) async-start(bf16[8,1,96,2048]{3,2,1,0:T(8,128)(2,1)} %fusion.87), calls=%async_computation.5 | async-start | bytes 6291456 | tf_op jit(solution)/shard_map/all_to_all | solution.py:187
  561.1 9.2 %copy-start.4 = (bf16[256,2048]{1,0:T(8,128)(2,1)S(1)}, bf16[256,2048]{1,0:T(8,128)(2,1)}, u32[]{:S(2)}) copy-start(bf16[256,2048]{1,0:T(8,128)(2,1)} %copy-done.3) | copy-start | bytes 3145732
  561.1 9.2 %copy-start.10 = (f32[2048]{0:T(1024)S(1)}, f32[2048]{0:T(1024)}, u32[]{:S(2)}) copy-start(f32[2048]{0:T(1024)} %param.45) | copy-start | bytes 24580
Sparse Core Ops, SparseCore 0:
  9.5 53.9 all-gather.9
  65.6 48.3 all-gather.7
  115.5 104.5 all-gather.5
where the time goes:
time: 586 us; the launch traced here: 579 us
  waiting for transfers between devices  187 us (32%)
  local copies, waits for them, and re-layouts  144 us (25%)
  blocking collectives  89 us (15%)
  matrix products  76.9 us (13%)
  other arithmetic  50.9 us (9%)
  starting transfers between devices  15.7 us (3%)
  between operations  14 us (2%)
    all_to_all x1, blocking collectives, local(): lax.all_to_all(send_rows, 'sp', split_axis=0, concat_axis=0, tiled=True)  74.7 us
    all_to_all x1, waiting for transfers between devices, local(): lax.all_to_all(expert_rows, 'sp', split_axis=0, concat_axis=0, tiled=True)  70.1 us
    all_gather x1, waiting for transfers between devices, local(): lax.all_gather(read_rows_input[0], 'sp', axis=0, tiled=True)  50.5 us
    all_to_all x1, waiting for transfers between devices, local(): lax.all_to_all(head_outputs, 'sp', split_axis=0, concat_axis=1, tiled=True)  36.6 us
    unnamed x43, local copies, waits for them, and re-layouts  29.6 us
    all_gather x1, waiting for transfers between devices, local(): lax.all_gather(write_rows_input[0], 'sp', axis=0, tiled=True)  24.9 us
    dot_general x16, matrix products, block_pass(): jnp.einsum('cls,csp->clp', weights, inp_block, preferred_element_type=jnp...  19.8 us
    all_to_all x1, blocking collectives, local(): lax.all_to_all(extra_log_decay[0], 'sp', split_axis=1, concat_axis=0, til...  14.2 us
  transfers between devices with their start and end apart: 7, of which 5 were waited for; matrix products, arithmetic and copies ran while one was open for 37% of the time, Pallas kernels for 0%

commit v1 on v0

v1 whole, which is shorter than its diff:
```python
import functools

import jax
import jax.numpy as jnp
from jax import lax
from jax.experimental import pallas as pl
from jax.experimental.pallas import tpu as pltpu
from jax.sharding import PartitionSpec as P

D = 2048
HEADS = 64
HEAD_DIM = 64
GROUPS = 2
STATE = 128
BLOCK = 128
TOPK = 2
INNER = 4096
PAD = 16


EPS = 1e-06


def rms_scale(values, scale_gain):
    return values * lax.rsqrt(jnp.mean(values * values, axis=-1, keepdims=True) + EPS) * scale_gain


def silu(values):
    return values / (1.0 + jnp.exp(-values))


def spread_pair(first, second, low_half):
    wide = (first.shape[0], BLOCK)
    return jnp.where(low_half, jnp.broadcast_to(first, wide), jnp.broadcast_to(second, wide))


def mixer_kernel(
    local_heads, x_ref, w_ref, r_ref, taps_ref, step_ref, decay_ref, step_t_ref, decay_t_ref,
    out_ref, padded, act, partial_y, cumul, state,
):
    length = out_ref.shape[0]
    width = out_ref.shape[1]
    blocks = length // BLOCK
    half = taps_ref.shape[0] // 2
    cols = width + 2 * STATE
    padded[0:PAD, :] = jnp.zeros((PAD, cols), jnp.bfloat16)
    padded[PAD + length : 2 * PAD + length, :] = jnp.zeros((PAD, cols), jnp.bfloat16)
    padded[PAD : PAD + length, 0:width] = x_ref[:, 0:width]
    padded[PAD : PAD + length, width : width + STATE] = w_ref[...]
    padded[PAD : PAD + length, width + STATE : cols] = r_ref[...]
    row_id = lax.broadcasted_iota(jnp.int32, (BLOCK, BLOCK), 0)
    col_id = lax.broadcasted_iota(jnp.int32, (BLOCK, BLOCK), 1)
    lower = row_id >= col_id
    diagonal = row_id == col_id
    tri = lower.astype(jnp.float32)
    tri_t = (row_id <= col_id).astype(jnp.float32)
    low_half = col_id < HEAD_DIM
    high = lax.Precision.HIGHEST

    state[...] = jnp.zeros_like(state)

    def forward(block, carry):
        start = pl.multiple_of(block * BLOCK, BLOCK)
        rows = pl.ds(start, BLOCK)
        for lo in range(0, cols, STATE):
            piece = padded[pl.ds(start, BLOCK + 2 * PAD), lo : lo + STATE].astype(jnp.float32)
            summed = jnp.zeros((BLOCK, STATE), jnp.float32)
            for offset in range(2 * half + 1):
                at = PAD - half + offset
                summed = summed + piece[at : at + BLOCK] * taps_ref[offset : offset + 1, lo : lo + STATE]
            act[rows, lo : lo + STATE] = silu(summed).astype(jnp.bfloat16)
        write = act[rows, width : width + STATE]
        read = act[rows, width + STATE : cols]
        decay = decay_ref[rows, :]
        cum = jnp.dot(tri, decay, precision=high, preferred_element_type=jnp.float32)
        cum_t = jnp.dot(
            decay_t_ref[:, rows], tri_t, precision=high, preferred_element_type=jnp.float32
        )
        before = cum - decay
        cumul[rows, :] = before
        before_t = cum_t - decay_t_ref[:, rows]
        step = step_ref[rows, :]
        step_t = step_t_ref[:, rows]
        scores = lax.dot_general(
            read, write, (((1,), (1,)), ((), ())), preferred_element_type=jnp.float32
        )
        entering = state[...].astype(jnp.bfloat16)
        carried = jnp.dot(read, entering, preferred_element_type=jnp.float32)
        scaled_parts = []
        leave_parts = []
        for pair in range(local_heads // 2):
            span = slice(pair * BLOCK, (pair + 1) * BLOCK)
            x_pair = act[rows, span]
            weights = []
            for h in (2 * pair, 2 * pair + 1):
                b = local_heads + h
                to_row = jnp.where(lower, cum[:, h : h + 1], -before[:, b : b + 1])
                from_col = jnp.where(lower, cum_t[h : h + 1, :], -before_t[b : b + 1, :])
                mult = jnp.where(lower, step_t[h : h + 1, :], step_t[b : b + 1, :])
                mult = mult + jnp.where(diagonal, step_t[b : b + 1, :], 0.0)
                weights.append(
                    (scores * jnp.exp(jnp.minimum(to_row - from_col, 0.0)) * mult).astype(jnp.bfloat16)
                )
            zero = jnp.zeros_like(x_pair)
            stacked = jnp.concatenate(
                [jnp.where(low_half, x_pair, zero), jnp.where(low_half, zero, x_pair)], axis=0
            )
            within = jnp.dot(
                jnp.concatenate(weights, axis=1), stacked, preferred_element_type=jnp.float32
            )
            h = 2 * pair
            cum_pair = spread_pair(cum[:, h : h + 1], cum[:, h + 1 : h + 2], low_half)
            step_pair = spread_pair(step[:, h : h + 1], step[:, h + 1 : h + 2], low_half)
            partial_y[rows, span] = within + carried[:, span] * jnp.exp(cum_pair)
            total = cum_pair[BLOCK - 1 : BLOCK, :]
            to_end = jnp.exp(total - cum_pair) * step_pair
            scaled_parts.append((x_pair.astype(jnp.float32) * to_end).astype(jnp.bfloat16))
            leave_parts.append(jnp.exp(total))
        scaled = jnp.concatenate(scaled_parts, axis=1)
        leaving = jnp.concatenate(leave_parts, axis=1)
        state[...] = state[...] * leaving + lax.dot_general(
            write, scaled, (((0,), (0,)), ((), ())), preferred_element_type=jnp.float32
        )
        return carry

    lax.fori_loop(0, blocks, forward, 0)
    state[...] = jnp.zeros_like(state)

    def backward(back, carry):
        block = blocks - 1 - back
        rows = pl.ds(pl.multiple_of(block * BLOCK, BLOCK), BLOCK)
        write = act[rows, width : width + STATE]
        read = act[rows, width + STATE : cols]
        before = cumul[rows, :]
        decay = decay_ref[rows, :]
        step = step_ref[rows, :]
        entering = state[...].astype(jnp.bfloat16)
        carried = jnp.dot(read, entering, preferred_element_type=jnp.float32)
        scaled_parts = []
        leave_parts = []
        for pair in range(local_heads // 2):
            span = slice(pair * BLOCK, (pair + 1) * BLOCK)
            x_pair = act[rows, span]
            b = local_heads + 2 * pair
            before_pair = spread_pair(before[:, b : b + 1], before[:, b + 1 : b + 2], low_half)
            step_pair = spread_pair(step[:, b : b + 1], step[:, b + 1 : b + 2], low_half)
            last = BLOCK - 1
            total = before_pair[last : last + 1, :] + spread_pair(
                decay[last : last + 1, b : b + 1],
                decay[last : last + 1, b + 1 : b + 2],
                low_half[0:1, :],
            )
            out_ref[rows, span] = (
                partial_y[rows, span] + carried[:, span] * jnp.exp(total - before_pair)
            ).astype(jnp.bfloat16)
            to_start = jnp.exp(before_pair) * step_pair
            scaled_parts.append((x_pair.astype(jnp.float32) * to_start).astype(jnp.bfloat16))
            leave_parts.append(jnp.exp(total))
        scaled = jnp.concatenate(scaled_parts, axis=1)
        leaving = jnp.concatenate(leave_parts, axis=1)
        state[...] = state[...] * leaving + lax.dot_general(
            write, scaled, (((0,), (0,)), ((), ())), preferred_element_type=jnp.float32
        )
        return carry

    lax.fori_loop(0, blocks, backward, 0)


def run_mixer(local_heads, x, write, read, taps, step, decay):
    length = x.shape[0]
    width = local_heads * HEAD_DIM
    cols = width + 2 * STATE
    vmem = pl.BlockSpec(memory_space=pltpu.VMEM)
    return pl.pallas_call(
        functools.partial(mixer_kernel, local_heads),
        out_shape=jax.ShapeDtypeStruct((length, width), jnp.bfloat16),
        in_specs=[vmem] * 8,
        out_specs=vmem,
        scratch_shapes=[
            pltpu.VMEM((length + 2 * PAD, cols), jnp.bfloat16),
            pltpu.VMEM((length, cols), jnp.bfloat16),
            pltpu.VMEM((length, width), jnp.float32),
            pltpu.VMEM((length, 2 * local_heads), jnp.float32),
            pltpu.VMEM((STATE, width), jnp.float32),
        ],
        compiler_params=pltpu.CompilerParams(vmem_limit_bytes=56 * 1024 * 1024),
        cost_estimate=pl.CostEstimate(
            flops=20 * length * width * BLOCK, bytes_accessed=8 * length * width, transcendentals=0
        ),
        name="mixer",
    )(x, write, read, taps, step, decay, step.T, decay.T)


def project_kernel(
    heads_ref, gate_ref, norm_gain_ref, matrix_ref, resid_ref, out_gain_ref, ffn_gain_ref,
    resid_one_ref, ffn_in_ref, normed, projected,
):
    step = pl.program_id(0)
    chunks, tok_rows, width = heads_ref.shape
    per_group = chunks // GROUPS

    @pl.when(step == 0)
    def _():
        for group in range(GROUPS):
            total = jnp.zeros((tok_rows, 1), jnp.float32)
            for i in range(group * per_group, (group + 1) * per_group):
                cols = slice(i * width, (i + 1) * width)
                u = heads_ref[i].astype(jnp.float32) * silu(gate_ref[:, cols].astype(jnp.float32))
                total = total + jnp.sum(u * u, axis=1, keepdims=True)
            scale = lax.rsqrt(total * (1.0 / (per_group * width)) + EPS)
            for i in range(group * per_group, (group + 1) * per_group):
                cols = slice(i * width, (i + 1) * width)
                u = heads_ref[i].astype(jnp.float32) * silu(gate_ref[:, cols].astype(jnp.float32))
                normed[:, cols] = (u * scale * norm_gain_ref[:, cols]).astype(jnp.bfloat16)

    parts, _, part = projected.shape
    projected[step] = jnp.dot(normed[...], matrix_ref[0], preferred_element_type=jnp.float32)

    @pl.when(step == pl.num_programs(0) - 1)
    def _():
        total = jnp.zeros((tok_rows, 1), jnp.float32)
        for j in range(parts):
            total = total + jnp.sum(projected[j] * projected[j], axis=1, keepdims=True)
        scale = lax.rsqrt(total * (1.0 / (parts * part)) + EPS)
        total = jnp.zeros((tok_rows, 1), jnp.float32)
        for j in range(parts):
            cols = slice(j * part, (j + 1) * part)
            one = (
                resid_ref[:, cols].astype(jnp.float32) + projected[j] * scale * out_gain_ref[:, cols]
            ).astype(jnp.bfloat16)
            resid_one_ref[:, cols] = one
            one = one.astype(jnp.float32)
            total = total + jnp.sum(one * one, axis=1, keepdims=True)
        scale = lax.rsqrt(total * (1.0 / (parts * part)) + EPS)
        for j in range(parts):
            cols = slice(j * part, (j + 1) * part)
            ffn_in_ref[:, cols] = (
                resid_one_ref[:, cols].astype(jnp.float32) * scale * ffn_gain_ref[:, cols]
            ).astype(jnp.bfloat16)


def run_project(heads, gate, norm_gain, matrix, resid, out_gain, ffn_gain):
    chunks, tok_rows, width = heads.shape
    parts, inner, part = matrix.shape
    model = parts * part

    def whole(shape):
        return pl.BlockSpec(shape, lambda j: (0,) * len(shape))

    return pl.pallas_call(
        project_kernel,
        grid=(parts,),
        out_shape=(
            jax.ShapeDtypeStruct((tok_rows, model), jnp.bfloat16),
            jax.ShapeDtypeStruct((tok_rows, model), jnp.bfloat16),
        ),
        in_specs=[
            whole(heads.shape),
            whole(gate.shape),
            whole((1, inner)),
            pl.BlockSpec((1, inner, part), lambda j: (j, 0, 0)),
            whole(resid.shape),
            whole((1, model)),
            whole((1, model)),
        ],
        out_specs=(whole((tok_rows, model)), whole((tok_rows, model))),
        scratch_shapes=[
            pltpu.VMEM((tok_rows, inner), jnp.bfloat16),
            pltpu.VMEM((parts, tok_rows, part), jnp.float32),
        ],
        compiler_params=pltpu.CompilerParams(vmem_limit_bytes=50 * 1024 * 1024),
        cost_estimate=pl.CostEstimate(
            flops=2 * tok_rows * inner * model, bytes_accessed=2 * inner * model, transcendentals=0
        ),
        name="project",
    )(heads, gate, norm_gain[None], matrix, resid, out_gain[None], ffn_gain[None])


def local(
    resid,
    mixer_inputs,
    output_gate,
    write_rows_input,
    read_rows_input,
    step_size_logits,
    extra_log_decay,
    mixer_conv_taps,
    write_conv_taps,
    read_conv_taps,
    step_size_bias,
    decay_speed,
    grouped_norm_gain,
    output_matrix,
    output_gain,
    feedforward_gain,
    routes,
    route_weights,
    expert_gate_weight,
    expert_up_weight,
    expert_down_weight,
    expert_sum_gain,
):
    tok_rows = mixer_inputs.shape[1]
    local_heads = step_size_bias.shape[0]
    per_group = HEADS // GROUPS
    width = local_heads * HEAD_DIM
    sp_size = lax.axis_size("sp")
    my_sp = lax.axis_index("sp")
    group_id = my_sp * local_heads // per_group
    gathered_rows = lax.all_gather(
        jnp.concatenate([write_rows_input[0], read_rows_input[0]], axis=1), "sp", axis=0, tiled=True
    )
    matrix_now, gathered_rows = lax.optimization_barrier((output_matrix, gathered_rows))
    matrix = lax.all_gather(matrix_now, "dp", axis=0, tiled=False)

    def by_dest(item):
        return jnp.moveaxis(item.reshape(tok_rows, sp_size, -1), 1, 0)

    def split_dirs(item):
        return jnp.moveaxis(
            item.reshape(tok_rows, sp_size, local_heads, 2), (1, 3), (0, 2)
        ).reshape(sp_size, tok_rows, 2 * local_heads)

    route_cols = jnp.broadcast_to(
        routes[0].astype(jnp.bfloat16)[None], (sp_size, tok_rows, TOPK)
    )
    sent = jnp.concatenate(
        [by_dest(mixer_inputs[0]), split_dirs(step_size_logits[0]), split_dirs(extra_log_decay[0]), route_cols],
        axis=2,
    )
    received = lax.all_to_all(sent, "sp", split_axis=0, concat_axis=0, tiled=True)
    received = received.reshape(sp_size * tok_rows, -1)
    dirs = 2 * local_heads
    step_pre = received[:, width : width + dirs].astype(jnp.float32)
    extra = received[:, width + dirs : width + 2 * dirs].astype(jnp.float32)
    routes_all = received[:, width + 2 * dirs :].astype(jnp.int32).reshape(sp_size, tok_rows, TOPK)
    step = jax.nn.softplus(step_pre + step_size_bias.T.reshape(1, dirs))
    decay = extra - decay_speed.T.reshape(1, dirs) * step
    col_start = group_id * STATE
    group_cols = GROUPS * STATE
    write_rows = lax.dynamic_slice_in_dim(gathered_rows, col_start, STATE, 1)
    read_rows = lax.dynamic_slice_in_dim(gathered_rows, group_cols + col_start, STATE, 1)
    taps = jnp.concatenate(
        [
            mixer_conv_taps,
            lax.dynamic_slice_in_dim(write_conv_taps, col_start, STATE, 1),
            lax.dynamic_slice_in_dim(read_conv_taps, col_start, STATE, 1),
        ],
        axis=1,
    ).astype(jnp.float32)
    head_outputs = run_mixer(local_heads, received, write_rows, read_rows, taps, step, decay)
    token_heads = lax.all_to_all(
        head_outputs.reshape(sp_size, tok_rows, width), "sp", split_axis=0, concat_axis=0, tiled=True
    )
    resid_one, ffn_in = run_project(
        token_heads, output_gate[0], grouped_norm_gain, matrix, resid[0], output_gain, feedforward_gain
    )
    local_experts = expert_gate_weight.shape[0]
    experts = local_experts * sp_size
    capacity = 3 * tok_rows * TOPK // (2 * experts)
    my_experts = my_sp * local_experts + jnp.arange(local_experts, dtype=jnp.int32)
    named = jnp.any(
        routes_all[:, None, :, :] == my_experts[None, :, None, None], axis=3
    ).astype(jnp.int32)
    place = jnp.where(named > 0, jnp.cumsum(named, axis=2) - 1, -1)
    slots = jnp.arange(capacity, dtype=jnp.int32)
    tokens = jnp.arange(tok_rows, dtype=jnp.int32)
    slot_token = jnp.sum(
        jnp.where(place[:, :, None, :] == slots[None, None, :, None], tokens, 0), axis=3
    )
    slot_row = slot_token + (jnp.arange(sp_size, dtype=jnp.int32) * tok_rows)[:, None, None]
    my_routes = routes[0]
    one_hot = (my_routes[:, :, None] == jnp.arange(experts, dtype=jnp.int32)).astype(jnp.int32)
    per_token = jnp.sum(one_hot, axis=1)
    earlier = jnp.cumsum(per_token, axis=0) - per_token
    slot_dest = my_routes * capacity + jnp.sum(earlier[:, None, :] * one_hot, axis=2)
    all_tokens = lax.all_gather(ffn_in, "sp", axis=0, tiled=True)
    arrived = all_tokens[slot_row.reshape(-1)].reshape(sp_size, local_experts, capacity, D)
    gate_part = jnp.einsum(
        "sekd,edh->sekh", arrived, expert_gate_weight, preferred_element_type=jnp.float32
    )
    up_part = jnp.einsum(
        "sekd,edh->sekh", arrived, expert_up_weight, preferred_element_type=jnp.float32
    )
    hidden = (jax.nn.silu(gate_part) * up_part).astype(jnp.bfloat16)
    expert_rows = jnp.einsum(
        "sekh,ehd->sekd", hidden, expert_down_weight, preferred_element_type=jnp.float32
    ).astype(jnp.bfloat16)
    returned = lax.all_to_all(expert_rows, "sp", split_axis=0, concat_axis=0, tiled=True)
    returned = returned.reshape(experts * capacity, D)
    combined = sum(
        returned[slot_dest[:, k]].astype(jnp.float32) * route_weights[0][:, k : k + 1]
        for k in range(TOPK)
    )
    mixed_out = resid_one.astype(jnp.float32) + rms_scale(combined, expert_sum_gain)
    return mixed_out.astype(jnp.bfloat16)[None]


def solution(mesh):
    in_specs = (
        P("dp", "sp", None),
        P("dp", "sp", None),
        P("dp", "sp", None),
        P("dp", "sp", None),
        P("dp", "sp", None),
        P("dp", "sp", None, None),
        P("dp", "sp", None, None),
        P(None, "sp"),
        P(),
        P(),
        P("sp", None),
        P("sp", None),
        P(),
        P(None, "dp"),
        P(),
        P(),
        P("dp", "sp", None),
        P("dp", "sp", None),
        P("sp", None, None),
        P("sp", None, None),
        P("sp", None, None),
        P(),
    )
    out_specs = P("dp", "sp", None)
    return jax.shard_map(local, mesh=mesh, in_specs=in_specs, out_specs=out_specs, check_vma=False)
```

time: 586 us -> 477 us (0.81); the launches traced: 579 us -> 476 us
  local copies, waits for them, and re-layouts: 144 us -> 34.5 us
  waiting for transfers between devices: 187 us -> 291 us
  matrix products: 76.9 us -> 20.8 us
  Pallas kernels: 0 us -> 46.5 us
  other arithmetic: 50.9 us -> 9.47 us
  blocking collectives: 89 us -> 52.4 us
  starting transfers between devices: 15.7 us -> 8.46 us
    all_gather x3, waiting for transfers between devices: 75.4 us -> 174 us  [the longest x1 121 us: local(): all_tokens = lax.all_gather(ffn_in, 'sp', axis=0, tiled=True)]
    dot_general x65 -> x0, matrix products: 58.7 us -> none  [the longest x16 19.8 us: block_pass(): jnp.einsum('cls,csp->clp', weights, inp_block, preferred_element_type=jnp...]
    pallas_call x0 -> x2, Pallas kernels: none -> 46.5 us  [the longest x1 32 us: run_mixer(): pl.pallas_call(functools.partial(mixer_kernel, local_heads), out_shape=ja...]
    all_to_all x2 -> x1, blocking collectives: 89 us -> 52.4 us  [local(): lax.all_to_all(head_outputs.reshape(sp_size, tok_rows, width), 'sp', spli...]
    rev x48 -> x0, local copies, waits for them, and re-layouts: 31 us -> none  [the longest x8 11.2 us: both_ways(): jnp.flip(inputs, 0)]
    unnamed x43 -> x35, local copies, waits for them, and re-layouts: 29.6 us -> 4.29 us
    convert_element_type x9 -> x2, other arithmetic: 17.7 us -> 0.62 us  [the longest x1 0.61 us: local(): taps = jnp.concatenate([mixer_conv_taps, lax.dynamic_slice_in_dim(write_c...]
    while x33 -> x0, local copies, waits for them, and re-layouts: 14.1 us -> none
  transfers between devices with their start and end apart: 7 -> 5, of which waited for: 5 -> 4; matrix products, arithmetic and copies ran while one was open for 37% -> 4% of each run, Pallas kernels for 0% -> 7%
where the time goes in v1:
time: 477 us; the launch traced here: 476 us
  waiting for transfers between devices  291 us (61%)
  blocking collectives  52.4 us (11%)
  Pallas kernels  46.5 us (10%)
  local copies, waits for them, and re-layouts  34.5 us (7%)
  matrix products  20.8 us (4%)
  between operations  13.5 us (3%)
  other arithmetic  9.47 us (2%)
  starting transfers between devices  8.46 us (2%)
    all_gather x1, waiting for transfers between devices, local(): all_tokens = lax.all_gather(ffn_in, 'sp', axis=0, tiled=True)  121 us
    all_to_all x1, waiting for transfers between devices, local(): lax.all_to_all(expert_rows, 'sp', split_axis=0, concat_axis=0, tiled=True)  69.2 us
    all_gather x1, waiting for transfers between devices, local(): lax.all_gather(jnp.concatenate([write_rows_input[0], read_rows_input[0]],...  53 us
    all_to_all x1, blocking collectives, local(): lax.all_to_all(head_outputs.reshape(sp_size, tok_rows, width), 'sp', spli...  52.4 us
    all_to_all x1, waiting for transfers between devices, local(): lax.all_to_all(sent, 'sp', split_axis=0, concat_axis=0, tiled=True)  47.2 us
    pallas_call x1, Pallas kernels, run_mixer(): pl.pallas_call(functools.partial(mixer_kernel, local_heads), out_shape=ja...  32 us
    pallas_call x1, Pallas kernels, run_project(): pl.pallas_call(project_kernel, grid=(parts,), out_shape=(jax.ShapeDtypeSt...  14.6 us
    dot_general x1, matrix products, local(): jnp.einsum('sekh,ehd->sekd', hidden, expert_down_weight, preferred_elemen...  12.6 us
  transfers between devices with their start and end apart: 5, of which 4 were waited for; matrix products, arithmetic and copies ran while one was open for 4% of the time, Pallas kernels for 7%

profile of v1, /device:TPU:0, one launch (start us, length us, event | category | flops | bytes accessed | tf_op | source)
XLA Modules:
  0.0 476.4 jit_solution(4493228045479201746)
XLA Ops:
  6.5 1.7 pad_maximum_fusion.1
  8.2 0.0 all-gather.5.cloned.1.call-update
  8.2 0.0 copy-start.8
  8.3 0.0 all-gather.9.cloned.1.call-start
  8.3 53.0 %all-gather.5.cloned.1.call-done = bf16[2048,512]{1,0:T(8,128)(2,1)} async-done(((bf16[256,512]{1,0:T(8,128)(2,1)}), bf16[2048,512]{1,0:T(8,128)(2,1)}) %all-gather.5.cloned.1.call-update) | async-done | bytes 2097168 | tf_op jit(solution)/shard_map/all_gather | solution.py:310
  61.3 0.0 all-gather.9.cloned.1.call-update
  61.3 3.3 copy.50
  64.7 1.5 pad_maximum_fusion
  66.3 0.0 copy-start.10
  66.3 3.8 all-to-all-start
  70.1 0.0 all-gather.7.cloned.1.call-start
  70.2 0.1 add.103
  70.3 0.1 mul.85
  70.4 0.6 maximum_convert_fusion.taps_ref
  71.0 2.6 constant_dynamic-slice_fusion.2
  73.5 47.2 %all-to-all-done = bf16[8,256,546]{1,2,0:T(8,128)(2,1)S(1)} async-done(((bf16[8,256,546]{1,2,0:T(8,128)(2,1)}), bf16[8,256,546]{1,2,0:T(8,128)(2,1)S(1)}, u32[]{:S(2)}, u32[]{:S(2)}) %all-to-all-start) | async-done | bytes 2236448 | tf_op jit(solution)/shard_map/all_to_all | solution.py:331
  120.8 0.5 copy.63
  121.2 0.1 pad.12
  121.4 0.8 copy.59
  122.2 2.8 copy.54.x_ref
  125.0 0.8 fusion.28
  125.8 1.3 copy.56.decay_ref
  127.1 1.3 copy.55.step_ref
  128.4 32.0 %mixer.1 = bf16[2048,512]{1,0:T(8,128)(2,1)} custom-call(bf16[2048,546]{1,0:T(8,128)(2,1)} %copy.54.x_ref, bf16[2048,128]{1,0:T(8,128)(2,1)} %get-tuple-element.17.w_ref, bf16[2048,128]{1,0:T(8,128)(2,1)} %get-tuple-element.16.r_ref, f32[5,768]{1,0:T(8,128)} %maximum_convert_fusion.taps_ref, f32[2048,16]{1,0:T(8,128)} %copy.55.step_ref, ...), custom_call_target="tpu_custom_call" | custom-call | flops 2684354560 | bytes 8388608 | tf_op jit(solution)/shard_map/mixer/pallas_call | solution.py:174
  160.4 52.4 %all_to_all.15.heads_ref = bf16[8,256,512]{2,1,0:T(8,128)(2,1)} all-to-all(bf16[8,256,512]{2,1,0:T(8,128)(2,1)} %bitcast.151), channel_id=1, replica_groups=mesh['sp'=8,'dp'=4] {'sp'}, dimensions={0} | all-to-all | bytes 4194304 | tf_op jit(solution)/shard_map/all_to_all | solution.py:352
  212.8 14.6 %project.1 = (bf16[256,2048]{1,0:T(8,128)(2,1)S(1)}, bf16[256,2048]{1,0:T(8,128)(2,1)}) custom-call(bf16[8,256,512]{2,1,0:T(8,128)(2,1)} %all_to_all.15.heads_ref, bf16[256,4096]{1,0:T(8,128)(2,1)} %bitcast.152, f32[1,4096]{1,0:T(1,128)S(1)} %bitcast.139, bf16[4,4096,512]{2,1,0:T(8,128)(2,1)} %bitcast.142, bf16[256,2048]{1,0:T(8,128)(2,1)S(1)} %bitcast.138, ...), custom_call_target="tpu_custom_call" | custom-call | flops 4294967296 | bytes 16777216 | tf_op jit(solution)/shard_map/project/pallas_call | solution.py:250
  227.4 0.0 all-gather.7.cloned.1.call-update
  227.4 0.1 add.107
  227.5 0.1 add.108
  227.6 0.8 compare_reduce_fusion
  228.4 0.6 reduce-window.14
  229.0 0.2 slice_reduce_fusion.1
  229.3 0.1 fusion.25
  229.4 0.2 select_reduce_fusion
  229.6 0.1 reduce_sum.39
  229.7 121.2 %all-gather.7.cloned.1.call-done = bf16[2048,2048]{1,0:T(8,128)(2,1)} async-done(((bf16[256,2048]{1,0:T(8,128)(2,1)}), bf16[2048,2048]{1,0:T(8,128)(2,1)}) %all-gather.7.cloned.1.call-update) | async-done | bytes 8388624 | tf_op jit(solution)/shard_map/all_gather | solution.py:377
  350.9 11.6 %gather_fusion = bf16[768,2048]{1,0:T(8,128)(2,1)} fusion(bf16[2048,2048]{1,0:T(8,128)(2,1)} %all-gather.7.cloned.1.call-done, s32[1024]{0:T(1024)S(1)} %pad_clamp_fusion.2), kind=kCustom, calls=%fused_computation | custom fusion | bytes 6294528 | tf_op jit(solution)/shard_map/gather | solution.py:378
  362.5 8.2 %fusion.2 = f32[8,96,1024]{2,1,0:T(8,128)} fusion(bf16[8,96,2048]{2,1,0:T(8,128)(2,1)} %bitcast.149, bf16[1,2048,1024]{2,1,0:T(8,128)(2,1)} %param.41), kind=kOutput, calls=%fused_computation.5 | convolution fusion | flops 3221225472 | bytes 10485760 | tf_op jit(solution)/shard_map/sekd,edh->sekh/dot_general | solution.py:382
  370.7 12.6 %fusion.13 = bf16[8,1,96,2048]{3,2,1,0:T(8,128)(2,1)} fusion(bf16[1,1024,2048]{2,1,0:T(8,128)(2,1)} %param.42, f32[8,96,1024]{2,1,0:T(8,128)} %fusion.2, bf16[8,96,2048]{2,1,0:T(8,128)(2,1)} %bitcast.150, bf16[1,2048,1024]{2,1,0:T(8,128)(2,1)} %param.40), kind=kOutput, calls=%fused_computation.17 | convolution fusion | flops 6448742400 | bytes 17825792 | tf_op jit(solution)/shard_map/sekh,ehd->sekd/dot_general | solution.py:386
  383.3 4.6 all-to-all-start.2
  387.9 0.6 reduce-window.16
  388.5 0.2 slice_reduce_fusion
  388.8 0.1 bitcast_subtract_fusion
  388.9 69.2 %all-to-all-done.2 = bf16[8,1,96,2048]{3,2,1,0:T(8,128)(2,1)} async-done(((bf16[8,1,96,2048]{3,2,1,0:T(8,128)(2,1)}), bf16[8,1,96,2048]{3,2,1,0:T(8,128)(2,1)}, u32[]{:S(2)}, u32[]{:S(2)}) %all-to-all-start.2) | async-done | bytes 3145760 | tf_op jit(solution)/shard_map/all_to_all | solution.py:389
  458.2 4.7 gather_fusion.1
  462.9 4.7 gather_fusion.2
  467.5 0.6 multiply_reduce_fusion
  468.2 1.7 fusion.19
  (54 shorter events, 0.3 us)
Async XLA Ops:
  6.5 54.8 %all-gather.5.cloned.1.call-start = ((), (), s32[]{:S(2)}) async-start(), calls=%async_computation.3 | async-start | bytes 2359296 | tf_op jit(solution)/shard_map/all_gather | solution.py:310
  8.2 56.4 %copy-start.8 = (s32[1,256,2]{1,2,0:T(2,128)S(1)}, s32[1,256,2]{1,2,0:T(2,128)}, u32[]{:S(2)}) copy-start(s32[1,256,2]{1,2,0:T(2,128)} %param.38) | copy-start | bytes 6148
  8.3 204.5 %all-gather.9.cloned.1.call-start = ((), (), s32[]{:S(2)}) async-start(), calls=%async_computation.5 | async-start | bytes 20971520 | tf_op jit(solution)/shard_map/all_gather | solution.py:314
  61.3 3.4 copy-start.6
  61.3 3.4 copy-start.7
  66.3 3.9 copy-start.14
  66.3 4.0 copy-start.15
  66.3 4.1 copy-start.12
  66.3 4.1 copy-start.13
  66.3 4.1 copy-start.10
  66.3 54.5 %all-to-all-start = ((bf16[8,256,546]{1,2,0:T(8,128)(2,1)}), bf16[8,256,546]{1,2,0:T(8,128)(2,1)S(1)}, u32[]{:S(2)}, u32[]{:S(2)}) async-start(bf16[8,256,546]{1,2,0:T(8,128)(2,1)} %pad_maximum_fusion), calls=%async_computation | async-start | bytes 4521984 | tf_op jit(solution)/shard_map/all_to_all | solution.py:331
  70.1 280.8 %all-gather.7.cloned.1.call-start = ((), (), s32[]{:S(2)}) async-start(), calls=%async_computation.4 | async-start | bytes 9437184 | tf_op jit(solution)/shard_map/all_gather | solution.py:377
  122.1 5.0 %copy-start.4 = (bf16[69,8,8,256]{3,1,2,0:T(8,128)(2,1)}, bf16[69,8,8,256]{3,1,2,0:T(8,128)(2,1)S(1)}, u32[]{:S(2)}) copy-start(bf16[69,8,8,256]{3,1,2,0:T(8,128)(2,1)S(1)} %copy.59) | copy-start | bytes 6782980
  125.8 2.6 copy-start.5
  160.4 52.4 %copy-start = (bf16[1,256,2048]{2,1,0:T(8,128)(2,1)S(1)}, bf16[1,256,2048]{2,1,0:T(8,128)(2,1)}, u32[]{:S(2)}) copy-start(bf16[1,256,2048]{2,1,0:T(8,128)(2,1)} %param.22) | copy-start | bytes 3145732
  160.4 52.4 %copy-start.1 = (f32[4096]{0:T(1024)S(1)}, f32[4096]{0:T(1024)}, u32[]{:S(2)}) copy-start(f32[4096]{0:T(1024)} %param.34) | copy-start | bytes 49156
  160.4 52.4 %copy-start.2 = (f32[2048]{0:T(1024)S(1)}, f32[2048]{0:T(1024)}, u32[]{:S(2)}) copy-start(f32[2048]{0:T(1024)} %param.36) | copy-start | bytes 24580
  160.4 52.4 %copy-start.3 = (f32[2048]{0:T(1024)S(1)}, f32[2048]{0:T(1024)}, u32[]{:S(2)}) copy-start(f32[2048]{0:T(1024)} %param.37) | copy-start | bytes 24580
  383.3 5.6 %copy-start.11 = (f32[1,256,2]{1,2,0:T(2,128)S(1)}, f32[1,256,2]{1,2,0:T(2,128)}, u32[]{:S(2)}) copy-start(f32[1,256,2]{1,2,0:T(2,128)} %param.39) | copy-start | bytes 6148
  383.3 74.9 %all-to-all-start.2 = ((bf16[8,1,96,2048]{3,2,1,0:T(8,128)(2,1)}), bf16[8,1,96,2048]{3,2,1,0:T(8,128)(2,1)}, u32[]{:S(2)}, u32[]{:S(2)}) async-start(bf16[8,1,96,2048]{3,2,1,0:T(8,128)(2,1)} %fusion.13), calls=%async_computation.2 | async-start | bytes 6291456 | tf_op jit(solution)/shard_map/all_to_all | solution.py:389
  462.8 5.3 %copy-start.9 = (f32[2048]{0:T(1024)S(1)}, f32[2048]{0:T(1024)}, u32[]{:S(2)}) copy-start(f32[2048]{0:T(1024)} %param.43) | copy-start | bytes 24580
Sparse Core Ops, SparseCore 0:
  9.5 51.7 all-gather.4
  62.9 104.4 all-gather.8
  227.6 123.3 all-gather.6

commit v2 on v1

--- a/solution.py
+++ b/solution.py
@@ -6,6 +6,7 @@
 from jax.experimental import pallas as pl
 from jax.experimental.pallas import tpu as pltpu
 from jax.sharding import PartitionSpec as P
+
 
 D = 2048
 HEADS = 64
@@ -14,7 +15,6 @@
 STATE = 128
 BLOCK = 128
 TOPK = 2
-INNER = 4096
 PAD = 16
 
 
@@ -35,7 +35,7 @@
 
 
 def mixer_kernel(
-    local_heads, x_ref, w_ref, r_ref, taps_ref, step_ref, decay_ref, step_t_ref, decay_t_ref,
+    local_heads, x_ref, rows_ref, taps_ref, step_ref, decay_ref, step_t_ref, decay_t_ref,
     out_ref, padded, act, partial_y, cumul, state,
 ):
     length = out_ref.shape[0]
@@ -46,8 +46,7 @@
     padded[0:PAD, :] = jnp.zeros((PAD, cols), jnp.bfloat16)
     padded[PAD + length : 2 * PAD + length, :] = jnp.zeros((PAD, cols), jnp.bfloat16)
     padded[PAD : PAD + length, 0:width] = x_ref[:, 0:width]
-    padded[PAD : PAD + length, width : width + STATE] = w_ref[...]
-    padded[PAD : PAD + length, width + STATE : cols] = r_ref[...]
+    padded[PAD : PAD + length, width:cols] = rows_ref[:, width:cols]
     row_id = lax.broadcasted_iota(jnp.int32, (BLOCK, BLOCK), 0)
     col_id = lax.broadcasted_iota(jnp.int32, (BLOCK, BLOCK), 1)
     lower = row_id >= col_id
@@ -166,7 +165,7 @@
     lax.fori_loop(0, blocks, backward, 0)
 
 
-def run_mixer(local_heads, x, write, read, taps, step, decay):
+def run_mixer(local_heads, x, rows, taps, step, decay):
     length = x.shape[0]
     width = local_heads * HEAD_DIM
     cols = width + 2 * STATE
@@ -174,7 +173,7 @@
     return pl.pallas_call(
         functools.partial(mixer_kernel, local_heads),
         out_shape=jax.ShapeDtypeStruct((length, width), jnp.bfloat16),
-        in_specs=[vmem] * 8,
+        in_specs=[vmem] * 7,
         out_specs=vmem,
         scratch_shapes=[
             pltpu.VMEM((length + 2 * PAD, cols), jnp.bfloat16),
@@ -188,29 +187,31 @@
             flops=20 * length * width * BLOCK, bytes_accessed=8 * length * width, transcendentals=0
         ),
         name="mixer",
-    )(x, write, read, taps, step, decay, step.T, decay.T)
+    )(x, rows, taps, step, decay, step.T, decay.T)
 
 
 def project_kernel(
-    heads_ref, gate_ref, norm_gain_ref, matrix_ref, resid_ref, out_gain_ref, ffn_gain_ref,
+    first_ref, second_ref, gate_ref, norm_gain_ref, matrix_ref, resid_ref, out_gain_ref, ffn_gain_ref,
     resid_one_ref, ffn_in_ref, normed, projected,
 ):
     step = pl.program_id(0)
-    chunks, tok_rows, width = heads_ref.shape
+    chunks, tok_rows, width = first_ref.shape
     per_group = chunks // GROUPS
 
     @pl.when(step == 0)
     def _():
         for group in range(GROUPS):
             total = jnp.zeros((tok_rows, 1), jnp.float32)
-            for i in range(group * per_group, (group + 1) * per_group):
+            for i in range(2 * group * per_group, 2 * (group + 1) * per_group):
                 cols = slice(i * width, (i + 1) * width)
-                u = heads_ref[i].astype(jnp.float32) * silu(gate_ref[:, cols].astype(jnp.float32))
+                heads_ref = (first_ref, second_ref)[i % 2]
+                u = heads_ref[i // 2].astype(jnp.float32) * silu(gate_ref[:, cols].astype(jnp.float32))
                 total = total + jnp.sum(u * u, axis=1, keepdims=True)
-            scale = lax.rsqrt(total * (1.0 / (per_group * width)) + EPS)
-            for i in range(group * per_group, (group + 1) * per_group):
+            scale = lax.rsqrt(total * (1.0 / (2 * per_group * width)) + EPS)
+            for i in range(2 * group * per_group, 2 * (group + 1) * per_group):
                 cols = slice(i * width, (i + 1) * width)
-                u = heads_ref[i].astype(jnp.float32) * silu(gate_ref[:, cols].astype(jnp.float32))
+                heads_ref = (first_ref, second_ref)[i % 2]
+                u = heads_ref[i // 2].astype(jnp.float32) * silu(gate_ref[:, cols].astype(jnp.float32))
                 normed[:, cols] = (u * scale * norm_gain_ref[:, cols]).astype(jnp.bfloat16)
 
     parts, _, part = projected.shape
@@ -239,8 +240,8 @@
             ).astype(jnp.bfloat16)
 
 
-def run_project(heads, gate, norm_gain, matrix, resid, out_gain, ffn_gain):
-    chunks, tok_rows, width = heads.shape
+def run_project(heads, others, gate, norm_gain, matrix, resid, out_gain, ffn_gain):
+    _, tok_rows, _ = heads.shape
     parts, inner, part = matrix.shape
     model = parts * part
 
@@ -256,6 +257,7 @@
         ),
         in_specs=[
             whole(heads.shape),
+            whole(others.shape),
             whole(gate.shape),
             whole((1, inner)),
             pl.BlockSpec((1, inner, part), lambda j: (j, 0, 0)),
@@ -273,7 +275,7 @@
             flops=2 * tok_rows * inner * model, bytes_accessed=2 * inner * model, transcendentals=0
         ),
         name="project",
-    )(heads, gate, norm_gain[None], matrix, resid, out_gain[None], ffn_gain[None])
+    )(heads, others, gate, norm_gain[None], matrix, resid, out_gain[None], ffn_gain[None])
 
 
 def local(
@@ -307,75 +309,76 @@
     sp_size = lax.axis_size("sp")
     my_sp = lax.axis_index("sp")
     group_id = my_sp * local_heads // per_group
-    gathered_rows = lax.all_gather(
-        jnp.concatenate([write_rows_input[0], read_rows_input[0]], axis=1), "sp", axis=0, tiled=True
-    )
-    matrix_now, gathered_rows = lax.optimization_barrier((output_matrix, gathered_rows))
-    matrix = lax.all_gather(matrix_now, "dp", axis=0, tiled=False)
-
-    def by_dest(item):
-        return jnp.moveaxis(item.reshape(tok_rows, sp_size, -1), 1, 0)
-
-    def split_dirs(item):
-        return jnp.moveaxis(
-            item.reshape(tok_rows, sp_size, local_heads, 2), (1, 3), (0, 2)
-        ).reshape(sp_size, tok_rows, 2 * local_heads)
-
-    route_cols = jnp.broadcast_to(
-        routes[0].astype(jnp.bfloat16)[None], (sp_size, tok_rows, TOPK)
-    )
-    sent = jnp.concatenate(
-        [by_dest(mixer_inputs[0]), split_dirs(step_size_logits[0]), split_dirs(extra_log_decay[0]), route_cols],
-        axis=2,
-    )
-    received = lax.all_to_all(sent, "sp", split_axis=0, concat_axis=0, tiled=True)
-    received = received.reshape(sp_size * tok_rows, -1)
-    dirs = 2 * local_heads
-    step_pre = received[:, width : width + dirs].astype(jnp.float32)
-    extra = received[:, width + dirs : width + 2 * dirs].astype(jnp.float32)
-    routes_all = received[:, width + 2 * dirs :].astype(jnp.int32).reshape(sp_size, tok_rows, TOPK)
-    step = jax.nn.softplus(step_pre + step_size_bias.T.reshape(1, dirs))
-    decay = extra - decay_speed.T.reshape(1, dirs) * step
+    matrix = lax.all_gather(output_matrix, "dp", axis=0, tiled=False)
+
+    def by_group(item):
+        grouped = jnp.moveaxis(item.reshape(tok_rows, GROUPS, STATE), 1, 0)
+        return jnp.repeat(grouped, sp_size // GROUPS, axis=0)
+
+    part_heads = local_heads // 2
+    part_width = part_heads * HEAD_DIM
+    dirs = 2 * part_heads
     col_start = group_id * STATE
-    group_cols = GROUPS * STATE
-    write_rows = lax.dynamic_slice_in_dim(gathered_rows, col_start, STATE, 1)
-    read_rows = lax.dynamic_slice_in_dim(gathered_rows, group_cols + col_start, STATE, 1)
-    taps = jnp.concatenate(
-        [
-            mixer_conv_taps,
-            lax.dynamic_slice_in_dim(write_conv_taps, col_start, STATE, 1),
-            lax.dynamic_slice_in_dim(read_conv_taps, col_start, STATE, 1),
-        ],
-        axis=1,
-    ).astype(jnp.float32)
-    head_outputs = run_mixer(local_heads, received, write_rows, read_rows, taps, step, decay)
-    token_heads = lax.all_to_all(
-        head_outputs.reshape(sp_size, tok_rows, width), "sp", split_axis=0, concat_axis=0, tiled=True
-    )
+    row_taps = [
+        lax.dynamic_slice_in_dim(item, col_start, STATE, 1) for item in (write_conv_taps, read_conv_taps)
+    ]
+
+    def to_send(part, rows):
+        heads = slice(part * part_heads, (part + 1) * part_heads)
+        small = [
+            jnp.moveaxis(
+                item[0].reshape(tok_rows, sp_size, local_heads, 2)[:, :, heads], (1, 3), (0, 2)
+            ).reshape(sp_size, tok_rows, dirs)
+            for item in (step_size_logits, extra_log_decay)
+        ]
+        channels = mixer_inputs[0].reshape(tok_rows, sp_size, width)
+        channels = channels[:, :, part * part_width : (part + 1) * part_width]
+        return jnp.concatenate([jnp.moveaxis(channels, 1, 0), *rows, *small], axis=2)
+
+    def mix(part, received, rows):
+        heads = slice(part * part_heads, (part + 1) * part_heads)
+        small = received[:, received.shape[1] - 2 * dirs :].astype(jnp.float32)
+        step = jax.nn.softplus(small[:, :dirs] + step_size_bias[heads].T.reshape(1, dirs))
+        decay = small[:, dirs:] - decay_speed[heads].T.reshape(1, dirs) * step
+        part_taps = mixer_conv_taps[:, part * part_width : (part + 1) * part_width]
+        taps = jnp.concatenate([part_taps, *row_taps], axis=1).astype(jnp.float32)
+        mixed = run_mixer(part_heads, received, rows, taps, step, decay)
+        return mixed.reshape(sp_size, tok_rows, part_width)
+
+    def exchange(item):
+        return lax.all_to_all(item, "sp", split_axis=0, concat_axis=0, tiled=True)
+
+    sent_first = to_send(0, [by_group(write_rows_input[0]), by_group(read_rows_input[0])])
+    sent_second = to_send(1, [])
+    first = exchange(sent_first)
+    first, sent_second = lax.optimization_barrier((first, sent_second))
+    second = exchange(sent_second).reshape(sp_size * tok_rows, -1)
+    first = first.reshape(sp_size * tok_rows, -1)
+    mixed_first = mix(0, first, first)
+    second, mixed_first = lax.optimization_barrier((second, mixed_first))
+    heads_first = exchange(mixed_first)
+    mixed_second = mix(1, second, first)
+    heads_second = exchange(mixed_second)
     resid_one, ffn_in = run_project(
-        token_heads, output_gate[0], grouped_norm_gain, matrix, resid[0], output_gain, feedforward_gain
+        heads_first, heads_second, output_gate[0], grouped_norm_gain, matrix, resid[0], output_gain, feedforward_gain
     )
     local_experts = expert_gate_weight.shape[0]
     experts = local_experts * sp_size
     capacity = 3 * tok_rows * TOPK // (2 * experts)
-    my_experts = my_sp * local_experts + jnp.arange(local_experts, dtype=jnp.int32)
-    named = jnp.any(
-        routes_all[:, None, :, :] == my_experts[None, :, None, None], axis=3
-    ).astype(jnp.int32)
-    place = jnp.where(named > 0, jnp.cumsum(named, axis=2) - 1, -1)
-    slots = jnp.arange(capacity, dtype=jnp.int32)
-    tokens = jnp.arange(tok_rows, dtype=jnp.int32)
-    slot_token = jnp.sum(
-        jnp.where(place[:, :, None, :] == slots[None, None, :, None], tokens, 0), axis=3
-    )
-    slot_row = slot_token + (jnp.arange(sp_size, dtype=jnp.int32) * tok_rows)[:, None, None]
     my_routes = routes[0]
     one_hot = (my_routes[:, :, None] == jnp.arange(experts, dtype=jnp.int32)).astype(jnp.int32)
     per_token = jnp.sum(one_hot, axis=1)
     earlier = jnp.cumsum(per_token, axis=0) - per_token
     slot_dest = my_routes * capacity + jnp.sum(earlier[:, None, :] * one_hot, axis=2)
-    all_tokens = lax.all_gather(ffn_in, "sp", axis=0, tiled=True)
-    arrived = all_tokens[slot_row.reshape(-1)].reshape(sp_size, local_experts, capacity, D)
+    named = per_token.T
+    place = jnp.where(named > 0, earlier.T, -1)
+    slots = jnp.arange(capacity, dtype=jnp.int32)
+    tokens = jnp.arange(tok_rows, dtype=jnp.int32)
+    slot_token = jnp.sum(
+        jnp.where(place[:, None, :] == slots[None, :, None], tokens, 0), axis=2
+    )
+    send_rows = ffn_in[slot_token.reshape(-1)].reshape(sp_size, local_experts, capacity, D)
+    arrived = lax.all_to_all(send_rows, "sp", split_axis=0, concat_axis=0, tiled=True)
     gate_part = jnp.einsum(
         "sekd,edh->sekh", arrived, expert_gate_weight, preferred_element_type=jnp.float32
     )

time: 477 us -> 401 us (0.84)
  waiting for transfers between devices: 291 us -> 141 us
  blocking collectives: 52.4 us -> 106 us
  Pallas kernels: 46.5 us -> 58.9 us
  starting transfers between devices: 8.46 us -> 19.5 us
    all_gather x3 -> x1, waiting for transfers between devices: 174 us -> 0.01 us  [local(): matrix = lax.all_gather(output_matrix, 'dp', axis=0, tiled=False)]
    all_to_all x1 -> x2, blocking collectives: 52.4 us -> 106 us  [the longest x1 74.5 us: local(): lax.all_to_all(send_rows, 'sp', split_axis=0, concat_axis=0, tiled=True)]
    all_to_all x1 -> x3, waiting for transfers between devices: 47.2 us -> 71 us  [exchange(): return lax.all_to_all(item, 'sp', split_axis=0, concat_axis=0, tiled=True)]
    pallas_call x1 -> x2, Pallas kernels: 32 us -> 45.1 us  [run_mixer(): pl.pallas_call(functools.partial(mixer_kernel, local_heads), out_shape=ja...]
    all_to_all x1 -> x3, starting transfers between devices: 3.8 us -> 14.7 us  [exchange(): return lax.all_to_all(item, 'sp', split_axis=0, concat_axis=0, tiled=True)]
    gather x1, local copies, waits for them, and re-layouts: 11.6 us -> 4.29 us  [local(): ffn_in[slot_token.reshape(-1)].reshape(sp_size, local_experts, capacity, D)]
  transfers between devices with their start and end apart: 5 -> 5, of which waited for: 4 -> 3; matrix products, arithmetic and copies ran while one was open for 4% -> 6% of each run, Pallas kernels for 7% -> 11%
where the time goes in v2:
time: 401 us; the launch traced here: 400 us
  waiting for transfers between devices  141 us (35%)
  blocking collectives  106 us (26%)
  Pallas kernels  58.9 us (15%)
  local copies, waits for them, and re-layouts  37.4 us (9%)
  starting transfers between devices  19.5 us (5%)
  matrix products  17.7 us (4%)
  between operations  13.8 us (3%)
  other arithmetic  5.34 us (1%)
    all_to_all x1, blocking collectives, local(): lax.all_to_all(send_rows, 'sp', split_axis=0, concat_axis=0, tiled=True)  74.5 us
    all_to_all x3, waiting for transfers between devices, exchange(): return lax.all_to_all(item, 'sp', split_axis=0, concat_axis=0, tiled=True)  71 us
    all_to_all x1, waiting for transfers between devices, local(): lax.all_to_all(expert_rows, 'sp', split_axis=0, concat_axis=0, tiled=True)  69.7 us
    pallas_call x2, Pallas kernels, run_mixer(): pl.pallas_call(functools.partial(mixer_kernel, local_heads), out_shape=ja...  45.1 us
    all_to_all x1, blocking collectives, exchange(): return lax.all_to_all(item, 'sp', split_axis=0, concat_axis=0, tiled=True)  31.7 us
    all_to_all x3, starting transfers between devices, exchange(): return lax.all_to_all(item, 'sp', split_axis=0, concat_axis=0, tiled=True)  14.7 us
    pallas_call x1, Pallas kernels, run_project(): pl.pallas_call(project_kernel, grid=(parts,), out_shape=(jax.ShapeDtypeSt...  13.7 us
    dot_general x1, matrix products, local(): jnp.einsum('sekh,ehd->sekd', hidden, expert_down_weight, preferred_elemen...  12.6 us
  transfers between devices with their start and end apart: 5, of which 3 were waited for; matrix products, arithmetic and copies ran while one was open for 6% of the time, Pallas kernels for 11%

profile of v2, /device:TPU:0, one launch (start us, length us, event | category | flops | bytes accessed | tf_op | source)
XLA Modules:
  0.0 400.1 jit_solution(13939756352070231641)
XLA Ops:
  6.5 0.7 all-gather.3.cloned.1.call-update
  7.3 0.1 copy-done.12
  7.5 3.3 copy.80
  10.9 0.1 copy.81
  11.1 0.1 copy.82
  11.3 1.2 fusion.32
  12.6 0.9 constant_dynamic-update-slice_fusion.3
  13.5 0.9 constant_dynamic-update-slice_fusion.2
  14.4 0.6 constant_dynamic-update-slice_fusion.1
  15.0 0.6 constant_dynamic-update-slice_fusion
  15.6 7.3 %all-to-all-start = ((bf16[8,256,528]{1,2,0:T(8,128)(2,1)}), bf16[8,256,528]{1,2,0:T(8,128)(2,1)S(1)}, u32[]{:S(2)}, u32[]{:S(2)}) async-start(bf16[8,256,528]{1,2,0:T(8,128)(2,1)} %constant_dynamic-update-slice_fusion), calls=%async_computation | async-start | bytes 4325376 | tf_op jit(solution)/shard_map/all_to_all | solution.py:349
  22.9 1.6 slice_bitcast_fusion
  24.6 1.1 pad_maximum_fusion
  25.7 46.9 %all-to-all-done = bf16[8,256,528]{1,2,0:T(8,128)(2,1)S(1)} async-done(((bf16[8,256,528]{1,2,0:T(8,128)(2,1)}), bf16[8,256,528]{1,2,0:T(8,128)(2,1)S(1)}, u32[]{:S(2)}, u32[]{:S(2)}) %all-to-all-start) | async-done | bytes 2162720 | tf_op jit(solution)/shard_map/all_to_all | solution.py:349
  72.6 3.6 all-to-all-start.1
  76.3 0.1 add.78
  76.4 0.1 mul.88
  76.7 0.6 fusion.34
  77.3 1.9 copy.104
  79.2 2.6 copy.89.x_ref.rows_ref
  81.8 0.1 slice_subtract_fusion.1
  81.9 1.3 copy.91.step_ref
  83.3 1.3 copy.92.decay_ref
  84.6 22.7 %mixer.2 = bf16[2048,256]{1,0:T(8,128)(2,1)} custom-call(bf16[2048,528]{1,0:T(8,128)(2,1)} %copy.89.x_ref.rows_ref, bf16[2048,528]{1,0:T(8,128)(2,1)} %copy.89.x_ref.rows_ref, f32[5,512]{1,0:T(8,128)} %get-tuple-element.28.taps_ref, f32[2048,8]{1,0:T(8,128)} %copy.91.step_ref, f32[2048,8]{1,0:T(8,128)} %copy.92.decay_ref, f32[8,2048]{1,0:T(8,128)} %bitcast.178, ...), custom_call_target="tpu_custom_call" | custom-call | flops 1342177280 | bytes 4194304 | tf_op jit(solution)/shard_map/mixer/pallas_call | solution.py:173
  107.3 0.1 copy.103
  107.4 1.5 copy.93.x_ref
  109.0 0.1 slice_subtract_fusion
  109.1 1.3 copy.95.step_ref
  110.4 1.3 copy.96.decay_ref
  111.8 22.4 %mixer.3 = bf16[2048,256]{1,0:T(8,128)(2,1)} custom-call(bf16[2048,272]{1,0:T(8,128)(2,1)} %copy.93.x_ref, bf16[2048,528]{1,0:T(8,128)(2,1)} %copy.89.x_ref.rows_ref, f32[5,512]{1,0:T(8,128)} %get-tuple-element.27.taps_ref, f32[2048,8]{1,0:T(8,128)} %copy.95.step_ref, f32[2048,8]{1,0:T(8,128)} %copy.96.decay_ref, f32[8,2048]{1,0:T(8,128)} %bitcast.176, ...), custom_call_target="tpu_custom_call" | custom-call | flops 1342177280 | bytes 4194304 | tf_op jit(solution)/shard_map/mixer/pallas_call | solution.py:173
  134.2 31.7 %all_to_all.30.second_ref = bf16[8,256,256]{2,1,0:T(8,128)(2,1)} all-to-all(bf16[8,256,256]{2,1,0:T(8,128)(2,1)} %bitcast.170), channel_id=1, replica_groups=mesh['sp'=8,'dp'=4] {'sp'}, dimensions={0} | all-to-all | bytes 2097152 | tf_op jit(solution)/shard_map/all_to_all | solution.py:349
  165.9 3.7 all-to-all-start.2
  169.6 0.6 reduce-window.6
  170.2 0.2 slice_reduce_fusion
  170.5 0.2 select_reduce_fusion
  170.9 24.1 %all-to-all-done.2.first_ref = bf16[8,256,256]{2,1,0:T(8,128)(2,1)S(1)} async-done(((bf16[8,256,256]{2,1,0:T(8,128)(2,1)}), bf16[8,256,256]{2,1,0:T(8,128)(2,1)S(1)}, u32[]{:S(2)}, u32[]{:S(2)}) %all-to-all-start.2) | async-done | bytes 1048608 | tf_op jit(solution)/shard_map/all_to_all | solution.py:349
  195.0 13.7 %project.1 = (bf16[256,2048]{1,0:T(8,128)(2,1)S(1)}, bf16[256,2048]{1,0:T(8,128)(2,1)S(1)}) custom-call(bf16[8,256,256]{2,1,0:T(8,128)(2,1)S(1)} %all-to-all-done.2.first_ref, bf16[8,256,256]{2,1,0:T(8,128)(2,1)} %all_to_all.30.second_ref, bf16[256,4096]{1,0:T(8,128)(2,1)} %bitcast.173, f32[1,4096]{1,0:T(1,128)S(1)} %bitcast.157, ...), custom_call_target="tpu_custom_call" | custom-call | flops 4294967296 | bytes 16777216 | tf_op jit(solution)/shard_map/project/pallas_call | solution.py:251
  208.7 4.3 %gather_fusion = bf16[768,2048]{1,0:T(8,128)(2,1)} fusion(bf16[256,2048]{1,0:T(8,128)(2,1)S(1)} %get-tuple-element.16, s32[1024]{0:T(1024)S(1)} %pad_clamp_fusion.2), kind=kCustom, calls=%fused_computation | custom fusion | bytes 6294528 | tf_op jit(solution)/shard_map/gather | solution.py:380
  213.0 74.5 %all_to_all.31 = bf16[8,1,96,2048]{3,2,1,0:T(8,128)(2,1)S(1)} all-to-all(bf16[8,1,96,2048]{3,2,1,0:T(8,128)(2,1)} %bitcast.161), channel_id=1, replica_groups=mesh['sp'=8,'dp'=4] {'sp'}, dimensions={0} | all-to-all | bytes 6291456 | tf_op jit(solution)/shard_map/all_to_all | solution.py:381
  287.5 1.7 copy-done.5
  289.3 5.1 %fusion.2 = f32[8,96,1024]{2,1,0:T(8,128)} fusion(bf16[1,2048,1024]{2,1,0:T(8,128)(2,1)S(1)} %copy-done.22, bf16[8,1,96,2048]{3,2,1,0:T(8,128)(2,1)S(1)} %all_to_all.31), kind=kOutput, calls=%fused_computation.5 | convolution fusion | flops 3221225472 | bytes 10485760 | tf_op jit(solution)/shard_map/sekd,edh->sekh/dot_general | solution.py:385
  294.4 12.6 %fusion.15 = bf16[8,1,96,2048]{3,2,1,0:T(8,128)(2,1)} fusion(bf16[1,1024,2048]{2,1,0:T(8,128)(2,1)} %param.42, f32[8,96,1024]{2,1,0:T(8,128)} %fusion.2, bf16[1,2048,1024]{2,1,0:T(8,128)(2,1)} %param.40, bf16[8,1,96,2048]{3,2,1,0:T(8,128)(2,1)} %copy-done.5), kind=kOutput, calls=%fused_computation.19 | convolution fusion | flops 6448742400 | bytes 17825792 | tf_op jit(solution)/shard_map/sekh,ehd->sekd/dot_general | solution.py:389
  306.9 4.8 %all-to-all-start.5 = ((bf16[8,1,96,2048]{3,2,1,0:T(8,128)(2,1)}), bf16[8,1,96,2048]{3,2,1,0:T(8,128)(2,1)}, u32[]{:S(2)}, u32[]{:S(2)}) async-start(bf16[8,1,96,2048]{3,2,1,0:T(8,128)(2,1)} %fusion.15), calls=%async_computation.5 | async-start | bytes 6291456 | tf_op jit(solution)/shard_map/all_to_all | solution.py:392
  311.9 69.7 %all-to-all-done.5 = bf16[8,1,96,2048]{3,2,1,0:T(8,128)(2,1)} async-done(((bf16[8,1,96,2048]{3,2,1,0:T(8,128)(2,1)}), bf16[8,1,96,2048]{3,2,1,0:T(8,128)(2,1)}, u32[]{:S(2)}, u32[]{:S(2)}) %all-to-all-start.5) | async-done | bytes 3145760 | tf_op jit(solution)/shard_map/all_to_all | solution.py:392
  381.5 4.7 %gather_fusion.1 = bf16[256,2048]{1,0:T(8,128)(2,1)S(1)} fusion(bf16[768,2048]{1,0:T(8,128)(2,1)} %bitcast.55, s32[1024]{0:T(1024)S(1)} %get-tuple-element.44), kind=kCustom, calls=%fused_computation.1 | custom fusion | bytes 2098176 | tf_op jit(solution)/shard_map/gather | solution.py:395
  386.2 4.7 %gather_fusion.2 = bf16[256,2048]{1,0:T(8,128)(2,1)S(1)} fusion(bf16[768,2048]{1,0:T(8,128)(2,1)} %bitcast.55, s32[1024]{0:T(1024)S(1)} %get-tuple-element.43), kind=kCustom, calls=%fused_computation.2 | custom fusion | bytes 2098176 | tf_op jit(solution)/shard_map/gather | solution.py:395
  390.9 0.6 multiply_reduce_fusion
  391.5 1.7 fusion.31
  (81 shorter events, 1.2 us)
Async XLA Ops:
  6.5 0.8 copy-start.12
  6.5 188.4 %all-gather.3.cloned.1.call-start = ((), (), s32[]{:S(2)}) async-start(), calls=%async_computation.6 | async-start | bytes 20971520 | tf_op jit(solution)/shard_map/all_gather | solution.py:312
  7.5 3.4 copy-start.10
  7.5 3.6 copy-start.11
  7.5 3.7 copy-start.13
  10.9 2.6 copy-start.4
  15.6 57.0 %all-to-all-start = ((bf16[8,256,528]{1,2,0:T(8,128)(2,1)}), bf16[8,256,528]{1,2,0:T(8,128)(2,1)S(1)}, u32[]{:S(2)}, u32[]{:S(2)}) async-start(bf16[8,256,528]{1,2,0:T(8,128)(2,1)} %constant_dynamic-update-slice_fusion), calls=%async_computation | async-start | bytes 4325376 | tf_op jit(solution)/shard_map/all_to_all | solution.py:349
  24.5 51.7 %copy-start.17 = (f32[8,2]{0,1:T(2,128)S(1)}, f32[8,2]{0,1:T(2,128)}, u32[]{:S(2)}) copy-start(f32[8,2]{0,1:T(2,128)} %param.32) | copy-start | bytes 196
  24.5 51.8 %copy-start.18 = (f32[8,2]{0,1:T(2,128)S(1)}, f32[8,2]{0,1:T(2,128)}, u32[]{:S(2)}) copy-start(f32[8,2]{0,1:T(2,128)} %param.33) | copy-start | bytes 196
  24.5 52.1 %copy-start.20 = (bf16[5,256]{1,0:T(8,128)(2,1)S(1)}, bf16[5,256]{1,0:T(8,128)(2,1)}, u32[]{:S(2)}) copy-start(bf16[5,256]{1,0:T(8,128)(2,1)} %param.31) | copy-start | bytes 7684
  24.6 52.1 %copy-start.21 = (bf16[5,256]{1,0:T(8,128)(2,1)S(1)}, bf16[5,256]{1,0:T(8,128)(2,1)}, u32[]{:S(2)}) copy-start(bf16[5,256]{1,0:T(8,128)(2,1)} %param.30) | copy-start | bytes 7684
  24.6 52.1 %copy-start.16 = (bf16[5,512]{1,0:T(8,128)(2,1)S(1)}, bf16[5,512]{1,0:T(8,128)(2,1)}, u32[]{:S(2)}) copy-start(bf16[5,512]{1,0:T(8,128)(2,1)} %param.29) | copy-start | bytes 15364
  72.6 4.8 %copy-start.3 = (bf16[8,256,528]{1,2,0:T(8,128)(2,1)}, bf16[8,256,528]{1,2,0:T(8,128)(2,1)S(1)}, u32[]{:S(2)}) copy-start(bf16[8,256,528]{1,2,0:T(8,128)(2,1)S(1)} %all-to-all-done) | copy-start | bytes 6488068
  72.6 34.7 %all-to-all-start.1 = ((bf16[8,256,272]{1,2,0:T(8,128)(2,1)}), bf16[8,256,272]{1,2,0:T(8,128)(2,1)S(1)}, u32[]{:S(2)}, u32[]{:S(2)}) async-start(bf16[8,256,272]{1,2,0:T(8,128)(2,1)} %pad_maximum_fusion), calls=%async_computation.1 | async-start | bytes 2228224 | tf_op jit(solution)/shard_map/all_to_all | solution.py:349
  81.9 2.7 copy-start.8
  81.9 2.6 copy-start.9
  109.1 2.6 copy-start.6
  109.1 2.6 copy-start.7
  134.2 35.4 %copy-start.14 = (s32[1,256,2]{1,2,0:T(2,128)S(1)}, s32[1,256,2]{1,2,0:T(2,128)}, u32[]{:S(2)}) copy-start(s32[1,256,2]{1,2,0:T(2,128)} %param.38) | copy-start | bytes 6148
  134.2 60.8 %copy-start = (f32[4096]{0:T(1024)S(1)}, f32[4096]{0:T(1024)}, u32[]{:S(2)}) copy-start(f32[4096]{0:T(1024)} %param.34) | copy-start | bytes 49156
  134.2 60.8 %copy-start.1 = (f32[2048]{0:T(1024)S(1)}, f32[2048]{0:T(1024)}, u32[]{:S(2)}) copy-start(f32[2048]{0:T(1024)} %param.36) | copy-start | bytes 24580
  134.2 60.8 %copy-start.2 = (f32[2048]{0:T(1024)S(1)}, f32[2048]{0:T(1024)}, u32[]{:S(2)}) copy-start(f32[2048]{0:T(1024)} %param.37) | copy-start | bytes 24580
  165.9 29.1 %all-to-all-start.2 = ((bf16[8,256,256]{2,1,0:T(8,128)(2,1)}), bf16[8,256,256]{2,1,0:T(8,128)(2,1)S(1)}, u32[]{:S(2)}, u32[]{:S(2)}) async-start(bf16[8,256,256]{2,1,0:T(8,128)(2,1)} %bitcast.17), calls=%async_computation.2 | async-start | bytes 2097152 | tf_op jit(solution)/shard_map/all_to_all | solution.py:349
  213.0 76.3 %copy-start.22 = (bf16[1,2048,1024]{2,1,0:T(8,128)(2,1)S(1)}, bf16[1,2048,1024]{2,1,0:T(8,128)(2,1)}, u32[]{:S(2)}) copy-start(bf16[1,2048,1024]{2,1,0:T(8,128)(2,1)} %param.41) | copy-start | bytes 12582916
  287.5 1.7 copy-start.5
  306.9 4.9 %copy-start.19 = (f32[1,256,2]{1,2,0:T(2,128)S(1)}, f32[1,256,2]{1,2,0:T(2,128)}, u32[]{:S(2)}) copy-start(f32[1,256,2]{1,2,0:T(2,128)} %param.39) | copy-start | bytes 6148
  306.9 74.6 %all-to-all-start.5 = ((bf16[8,1,96,2048]{3,2,1,0:T(8,128)(2,1)}), bf16[8,1,96,2048]{3,2,1,0:T(8,128)(2,1)}, u32[]{:S(2)}, u32[]{:S(2)}) async-start(bf16[8,1,96,2048]{3,2,1,0:T(8,128)(2,1)} %fusion.15), calls=%async_computation.5 | async-start | bytes 6291456 | tf_op jit(solution)/shard_map/all_to_all | solution.py:392
  386.2 5.3 %copy-start.15 = (f32[2048]{0:T(1024)S(1)}, f32[2048]{0:T(1024)}, u32[]{:S(2)}) copy-start(f32[2048]{0:T(1024)} %param.43) | copy-start | bytes 24580
Sparse Core Ops, SparseCore 0:
  8.9 108.6 all-gather.2
